TPU v7x, 1024 devices: a whole 4x8x16 slice. The times are simulated.
1024 devices in a mesh: sp: 128 (over z, y), tp: 8 (over x, core).
Axes of the slice: x: 4, y: 8, z: 16, core: 2. Of those that a mesh axis runs over, the one named last changes fastest.
Arguments:
- tokens: bfloat16 [49152, 2048], P('sp'), may hold values from -6 to 6
- in_gain: float32 [2048], replicated, may hold values from 0.1 to 1.9
- query_weight: bfloat16 [2048, 1024], P(None, 'tp'), may hold values from -0.125 to 0.125
- key_weight: bfloat16 [2048, 1024], P(None, 'tp'), may hold values from -0.125 to 0.125
- value_weight: bfloat16 [2048, 2048], P(None, 'tp'), may hold values from -0.125 to 0.125
- gate_weight: bfloat16 [2048, 2048], P(None, 'tp'), may hold values from -0.125 to 0.125
- decay_down: bfloat16 [2048, 32], replicated, may hold values from -0.125 to 0.125
- decay_up: bfloat16 [32, 1024], replicated, may hold values from -1 to 1
- decay_offset: float32 [1024], P('tp')
- decay_extra: float32 [49152, 1024], P('sp', 'tp'), may hold values from -2 to 0, as said below
- head_gain: float32 [2048], P('tp'), may hold values from 0.1 to 1.9
- out_weight: bfloat16 [2048, 2048], P(None, 'tp'), may hold values from -4 to 4
- out_gain: float32 [2048], P('tp'), may hold values from 0.1 to 1.9
Outputs:
- layer_output: bfloat16 [49152, 2048], P('sp', 'tp')
Inputs may be any that keep to these rules, and one draw needn't show every extreme that they name: `decay_extra`: never positive.
All inputs are finite; a program needn't handle non-finite values.
Results may differ from a plain program's by a relative error of at most 0.015.
Values may be sent and summed in bfloat16 or wider, within the bound.
A program may use at most 64 MiB of HBM per device.

v0:
```python
import jax
import jax.numpy as jnp
from jax import lax
from jax.sharding import Mesh
from jax.sharding import PartitionSpec as P

D = 2048
QUERY_FEATURES = 128
DV = 256
BLOCK = 64
SP = ("sp_0", "sp_1")


norm_eps = 1e-06
decay_temper = 16.0
highest = lax.Precision.HIGHEST


def filled_with(array, identity):
    return jax.tree.map(
        lambda a, e: jnp.broadcast_to(jnp.asarray(e, a.dtype), a.shape), array, identity
    )


def carried_in(array, axes, combine, identity):
    before = start = filled_with(array, identity)
    subtotal = array
    for axis in reversed(axes):
        length, index = (lax.axis_size(axis), lax.axis_index(axis))
        pieces = jax.tree.map(lambda part: lax.all_gather(part, axis), subtotal)
        inside, subtotal = (start, start)
        for k in range(length):
            passed = k < index
            subtotal = combine(subtotal, jax.tree.map(lambda part: part[k], pieces))
            inside = jax.tree.map(lambda new, old: jnp.where(passed, new, old), subtotal, inside)
        before = combine(inside, before)
    return before


def joined_along(parts, dim):
    parts = jnp.moveaxis(parts, 0, dim)
    lengths = parts.shape
    return parts.reshape(*lengths[:dim], lengths[dim] * lengths[dim + 1], *lengths[dim + 2 :])


def from_everyone(array, axis):
    copies = jnp.broadcast_to(array, (lax.axis_size(axis), *array.shape))
    return lax.all_to_all(copies, axis, split_axis=0, concat_axis=0, tiled=True)


def collect(array, axis, dim):
    return joined_along(from_everyone(array, axis), dim)


def of_everyone(array, axis):
    return from_everyone(array, axis).sum(axis=0)


def combine_states(earlier, latter):
    decay_first, state_first = earlier
    decay_second, state_second = latter
    return (decay_first * decay_second, decay_second[:, :, None] * state_first + state_second)


def block_pass(query_heads, key_heads, value_heads, decay_heads, state_start):
    row_count = query_heads.shape[0]
    block_count = row_count // BLOCK
    causal_mask = jnp.arange(BLOCK)[:, None] >= jnp.arange(BLOCK)[None, :]

    def to_blocks(values):
        return values.reshape(block_count, BLOCK, values.shape[1], values.shape[2])

    def block_step(carry_state, inputs):
        query_block, key_block, value_block, decay_block = inputs
        cumulative = jnp.cumsum(decay_block, axis=0)
        closing = cumulative[-1]
        query_inner = query_block * jnp.exp(cumulative)
        key_inner = key_block * jnp.exp(-cumulative)
        scores = jnp.einsum("chd,shd->hcs", query_inner, key_inner, precision=highest)
        scores = jnp.where(causal_mask[None], scores, 0.0)
        output = jnp.einsum("hcs,she->che", scores, value_block, precision=highest)
        output = output + jnp.einsum("chd,hde->che", query_inner, carry_state, precision=highest)
        key_closing = key_block * jnp.exp(closing[None] - cumulative)
        carry_state = carry_state * jnp.exp(closing)[:, :, None] + jnp.einsum(
            "chd,che->hde", key_closing, value_block, precision=highest
        )
        return (carry_state, output)

    state_end, outputs = lax.scan(
        block_step,
        state_start,
        (
            to_blocks(query_heads),
            to_blocks(key_heads),
            to_blocks(value_heads),
            to_blocks(decay_heads),
        ),
    )
    return (state_end, outputs.reshape(row_count, outputs.shape[2], outputs.shape[3]))


def link_scan(device_decay, local_state):
    decay_in, state_in = carried_in(
        (device_decay, local_state),
        SP,
        combine_states,
        (jnp.ones_like(device_decay), jnp.zeros_like(local_state)),
    )
    return state_in


def carry_heads(query_heads, key_heads, value_heads, decay_heads, link_chain):
    cumulative = jnp.cumsum(decay_heads, axis=0)
    device_decay = jnp.exp(cumulative[-1])
    key_closing = key_heads * jnp.exp(cumulative[-1][None] - cumulative)
    local_state = jnp.einsum("thd,the->hde", key_closing, value_heads, precision=highest)
    carried = link_chain(device_decay, local_state)
    final_state, result = block_pass(query_heads, key_heads, value_heads, decay_heads, carried)
    return result


def local(
    tokens,
    in_gain,
    query_weight,
    key_weight,
    value_weight,
    gate_weight,
    decay_down,
    decay_up,
    decay_offset,
    decay_extra,
    head_gain,
    out_weight,
    out_gain,
):
    row_count = tokens.shape[0]
    head_count = query_weight.shape[1] // QUERY_FEATURES
    tokens_wide = tokens.astype(jnp.float32)
    normed = (
        tokens_wide
        * lax.rsqrt(jnp.mean(tokens_wide * tokens_wide, axis=1, keepdims=True) + norm_eps)
        * in_gain
    ).astype(jnp.bfloat16)

    def project(weight):
        return jnp.dot(normed, weight, preferred_element_type=jnp.float32).astype(jnp.bfloat16)

    query_rows = project(query_weight)
    key_rows = project(key_weight)
    value_rows = project(value_weight)
    gate_rows = project(gate_weight)
    low_rank = project(decay_down)
    channel_count = decay_offset.shape[0]
    up_columns = lax.dynamic_slice_in_dim(
        decay_up, lax.axis_index("tp") * channel_count, channel_count, 1
    )
    logits = jnp.dot(low_rank, up_columns, preferred_element_type=jnp.float32)
    log_decay = jax.nn.log_sigmoid(logits + decay_offset) / decay_temper + decay_extra
    query_heads = query_rows.astype(jnp.float32).reshape(row_count, head_count, QUERY_FEATURES)
    key_heads = key_rows.astype(jnp.float32).reshape(row_count, head_count, QUERY_FEATURES)
    value_heads = value_rows.astype(jnp.float32).reshape(row_count, head_count, DV)
    decay_heads = log_decay.reshape(row_count, head_count, QUERY_FEATURES)
    attended = carry_heads(query_heads, key_heads, value_heads, decay_heads, link_scan)
    scaled = (
        attended
        * lax.rsqrt(jnp.mean(attended * attended, axis=2, keepdims=True) + norm_eps)
        * head_gain.reshape(head_count, DV)
    )
    gated = (
        scaled.reshape(row_count, head_count * DV) * jax.nn.silu(gate_rows.astype(jnp.float32))
    ).astype(jnp.bfloat16)
    mixed = jnp.dot(collect(gated, "tp", 1), out_weight, preferred_element_type=jnp.float32)
    squares = of_everyone(jnp.sum(mixed * mixed, axis=1), "tp")
    result = mixed * lax.rsqrt(squares[:, None] / D + norm_eps) * out_gain
    return result.astype(jnp.bfloat16)


def solution(mesh):
    torus = Mesh(mesh.devices.reshape(16, 8, mesh.shape["tp"]), ("sp_0", "sp_1", "tp"))
    in_specs = (
        P(SP, None),
        P(),
        P(None, "tp"),
        P(None, "tp"),
        P(None, "tp"),
        P(None, "tp"),
        P(),
        P(),
        P("tp"),
        P(SP, "tp"),
        P("tp"),
        P(None, "tp"),
        P("tp"),
    )
    out_specs = P(SP, "tp")
    return jax.shard_map(local, mesh=torus, in_specs=in_specs, out_specs=out_specs, check_vma=False)
```

profile of v0, /device:TPU:1, one launch (start us, length us, event | category | flops | bytes accessed | tf_op | source)
XLA Modules:
  0.0 216.7 jit_solution(15233167668903736525)
XLA Ops:
  6.5 1.9 fusion.30
  8.5 1.9 fusion.32
  10.4 1.6 fusion.43
  12.3 1.9 convolution_convert_fusion.1
  14.8 1.0 fusion.44
  15.9 13.8 %all_gather.18 = f32[8,1,128]{2,1,0:T(1,128)S(1)} all-gather(f32[1,1,128]{2,1,0:T(1,128)S(1)} %get-tuple-element.113), channel_id=1, replica_groups=mesh['sp_0'=16,'sp_1'=8,'tp'=8] {'sp_1'}, dimensions={0}, use_global_device_ids=true | all-gather | bytes 4608 | tf_op jit(solution)/shard_map/all_gather | solution.py:30
  30.2 35.5 %all-gather.6.cloned.1.call-done = f32[1024,256]{1,0:T(8,128)} async-done(((f32[128,256]{1,0:T(8,128)}), f32[1024,256]{1,0:T(8,128)}) %all-gather.6.cloned.1.call-update) | async-done | bytes 1048592 | tf_op jit(solution)/shard_map/all_gather | solution.py:30
  65.8 2.1 bitcast_add_fusion.9
  68.0 1.0 convert.2
  69.0 1.6 convolution_convert_fusion.2
  71.3 24.1 %all_gather.19 = f32[16,1,128]{2,1,0:T(1,128)S(1)} all-gather(f32[1,1,128]{2,1,0:T(1,128)S(1)} %get-tuple-element.133), channel_id=1, replica_groups=mesh['sp_0'=16,'sp_1'=8,'tp'=8] {'sp_0'}, dimensions={0}, use_global_device_ids=true | all-gather | bytes 8704 | tf_op jit(solution)/shard_map/all_gather | solution.py:30
  96.1 43.7 %all-gather.4.cloned.1.call-done = f32[16,1,128,256]{3,2,1,0:T(8,128)} async-done(((f32[1,1,128,256]{3,2,1,0:T(8,128)}), f32[16,1,128,256]{3,2,1,0:T(8,128)}) %all-gather.4.cloned.1.call-update) | async-done | bytes 2097168 | tf_op jit(solution)/shard_map/all_gather | solution.py:30
  139.8 2.5 %fusion.52 = f32[1,128,256]{2,1,0:T(8,128)S(1)} fusion(f32[16,1,128,256]{3,2,1,0:T(8,128)} %all-gather.4.cloned.1.call-done, f32[1024,256]{1,0:T(8,128)} %all-gather.6.cloned.1.call-done, f32[128]{0:T(128)} %copy-done.9, f32[128]{0:T(128)} %copy-done.8, f32[128]{0:T(128)} %copy-done.7, f32[128]{0:T(128)} %copy-done.6, f32[128]{0:T(128)S(1)} %get-tuple-element.137, ...), kind=kLoop, calls=%fused_computation.74 | loop fusion | flops 2359296 | bytes 3289624 | tf_op jit(solution)/shard_map/add | solution.py:62
  142.3 19.6 %while.13 = (s32[]{:T(128)}, f32[1,128,256]{2,1,0:T(8,128)S(1)}, f32[6,64,1,256]{3,1,2,0:T(8,128)}, f32[6,64,1,128]{3,1,2,0:T(8,128)S(1)}, f32[6,64,1,128]{3,1,2...) while((s32[]{:T(128)}, f32[1,128,256]{2,1,0:T(8,128)S(1)}, ...), condition=%wide.region_5.6_spmd.clone, body=%wide.region_3.5_spmd.clone.sunk | while | flops 69861376 | bytes 1169501 | solution.py:89
  143.6 1.6 fusion.123
  146.9 1.6 fusion.123
  150.1 1.6 fusion.123
  153.4 1.6 fusion.123
  156.7 1.6 fusion.123
  159.9 1.6 fusion.123
  161.9 1.1 multiply_reduce_fusion.1
  163.1 1.9 fusion.38
  165.4 34.7 %all_to_all.11 = bf16[8,384,256]{1,2,0:T(8,128)(2,1)S(1)} all-to-all(bf16[8,384,256]{1,2,0:T(8,128)(2,1)S(1)} %broadcast_in_dim.43), channel_id=1, replica_groups=mesh['sp_0'=16,'sp_1'=8,'tp'=8] {'tp'}, dimensions={0} | all-to-all | bytes 3145728 | tf_op jit(solution)/shard_map/all_to_all | solution.py:48
  200.9 8.0 %all_to_all.12 = f32[8,1,384]{2,1,0:T(1,128)S(1)} all-to-all(f32[8,1,384]{2,1,0:T(1,128)S(1)} %broadcast_in_dim.44), channel_id=1, replica_groups=mesh['sp_0'=16,'sp_1'=8,'tp'=8] {'tp'}, dimensions={0} | all-to-all | bytes 24576 | tf_op jit(solution)/shard_map/all_to_all | solution.py:48
  (97 shorter events, 14.6 us)
Async XLA Ops:
  6.5 193.6 %copy-start = (bf16[2048,256]{1,0:T(8,128)(2,1)S(1)}, bf16[2048,256]{1,0:T(8,128)(2,1)}, u32[]{:S(2)}) copy-start(bf16[2048,256]{1,0:T(8,128)(2,1)} %param.26) | copy-start | bytes 3145732
  6.5 1.9 copy-start.5
  6.5 59.2 %all-gather.6.cloned.1.call-start = ((), (), s32[]{:S(2)}) async-start(), calls=%async_computation.3 | async-start | bytes 1179648 | tf_op jit(solution)/shard_map/all_gather | solution.py:30
  8.4 1.9 copy-start.3
  8.5 1.9 copy-start.4
  8.5 1.9 copy-start.11
  12.3 1.9 copy-start.2
  14.2 1.6 copy-start.1
  15.8 124.0 %all-gather.4.cloned.1.call-start = ((), (), s32[]{:S(2)}) async-start(), calls=%async_computation.2 | async-start | bytes 2228224 | tf_op jit(solution)/shard_map/all_gather | solution.py:30
  29.7 38.3 %copy-start.6 = (f32[128]{0:T(128)}, f32[128]{0:T(128)S(1)}, u32[]{:S(2)}) copy-start(f32[128]{0:T(128)S(1)} %get-tuple-element.138) | copy-start | bytes 1540
  29.7 38.3 %copy-start.7 = (f32[128]{0:T(128)}, f32[128]{0:T(128)S(1)}, u32[]{:S(2)}) copy-start(f32[128]{0:T(128)S(1)} %get-tuple-element.139) | copy-start | bytes 1540
  29.7 38.3 %copy-start.8 = (f32[128]{0:T(128)}, f32[128]{0:T(128)S(1)}, u32[]{:S(2)}) copy-start(f32[128]{0:T(128)S(1)} %get-tuple-element.140) | copy-start | bytes 1540
  30.2 37.8 %copy-start.9 = (f32[128]{0:T(128)}, f32[128]{0:T(128)S(1)}, u32[]{:S(2)}) copy-start(f32[128]{0:T(128)S(1)} %get-tuple-element.132) | copy-start | bytes 1540
  142.3 20.8 %copy-start.12 = (f32[256]{0:T(256)S(1)}, f32[256]{0:T(256)}, u32[]{:S(2)}) copy-start(f32[256]{0:T(256)} %param.25) | copy-start | bytes 3076
  200.1 8.9 %copy-start.10 = (f32[256]{0:T(256)S(1)}, f32[256]{0:T(256)}, u32[]{:S(2)}) copy-start(f32[256]{0:T(256)} %param.27) | copy-start | bytes 3076
Sparse Core Ops, SparseCore 0:
  15.9 49.7 all-gather.5
  68.4 71.3 all-gather.3
where the time goes:
time: 218 us; the launch traced here: 217 us
  blocking collectives  80.7 us (37%)
  waiting for transfers between devices  79.3 us (36%)
  matrix products  28.1 us (13%)
  between operations  13.8 us (6%)
  other arithmetic  13.1 us (6%)
    all_gather x2, waiting for transfers between devices, carried_in(): pieces = jax.tree.map(lambda part: lax.all_gather(part, axis), subtotal)  79.3 us
    all_to_all x2, blocking collectives, from_everyone(): return lax.all_to_all(copies, axis, split_axis=0, concat_axis=0, tiled=True)  42.7 us
    all_gather x2, blocking collectives, carried_in(): pieces = jax.tree.map(lambda part: lax.all_gather(part, axis), subtotal)  38 us
    dot_general x6, matrix products, block_step(): jnp.einsum('chd,hde->che', query_inner, carry_state, precision=highest)  9.63 us
    dot_general x4, matrix products, project(): jnp.dot(normed, weight, preferred_element_type=jnp.float32)  5.94 us
    dot_general x6, matrix products, block_step(): jnp.einsum('chd,shd->hcs', query_inner, key_inner, precision=highest)  5.68 us
    add x2, other arithmetic, combine_states(): decay_second[:, :, None] * state_first + state_second  4.63 us
  transfers between devices with their start and end apart: 2, of which 2 were waited for; matrix products, arithmetic and copies ran while one was open for 2% of the time, Pallas kernels for 0%

commit v1 on v0

v1 whole, which is shorter than its diff:
```python
import functools

import jax
import jax.numpy as jnp
from jax import lax
from jax.experimental import pallas as pl
from jax.experimental.pallas import tpu as pltpu
from jax.sharding import Mesh
from jax.sharding import PartitionSpec as P

QUERY_FEATURES = 128
DV = 256
CHUNK = 128
NX = 4
norm_eps = 1e-06
decay_temper = 16.0
MESH = pl.DeviceIdType.MESH
f32 = jnp.float32
bf16 = jnp.bfloat16


def dot(a, b, ca=1, cb=0):
    return lax.dot_general(a, b, (((ca,), (cb,)), ((), ())), preferred_element_type=f32)


def dot_wide(a, b):
    a_hi, b_hi = a.astype(bf16), b.astype(bf16)
    a_lo, b_lo = (a - a_hi.astype(f32)).astype(bf16), (b - b_hi.astype(f32)).astype(bf16)
    return dot(jnp.concatenate([a_hi, a_hi, a_lo], axis=1), jnp.concatenate([b_hi, b_lo, b_hi], axis=1), 1, 1)


def far_first(n):
    return sorted(range(1, n), key=lambda o: -min(o, n - o))


def kernel(
    nz,
    ny,
    tok_h,
    ing_h,
    wq_h,
    wk_h,
    wv_h,
    wg_h,
    dd_h,
    du_h,
    off_h,
    ext_h,
    hg_h,
    wo_h,
    og_h,
    out_ref,
    tok,
    nrm,
    wq,
    wk,
    wv,
    wg,
    wo,
    dd,
    du,
    ing,
    doff,
    ext,
    hg,
    og,
    cum,
    kk,
    vv,
    qq,
    fac,
    qhat,
    att,
    st,
    gsend,
    arr,
    garr,
    inside,
    wbuf,
    tsend,
    gtsend,
    zarr,
    zgarr,
    bsend,
    sin,
    gat,
    acc,
    ssend,
    sarr,
    lsem,
    s1s,
    s1r,
    g1s,
    g1r,
    s2s,
    s2r,
    g2s,
    g2r,
    s3s,
    s3r,
    gs,
    gr,
    nss,
    nsr,
):
    z, y, x, c = (lax.axis_index(name) for name in ("z", "y", "x", "c"))
    rows, width = tok.shape
    half = rows // 2
    chunks = rows // CHUNK
    piece = DV // ny
    me = x * 2 + c
    plus, minus, across = lax.rem(x + 1, NX), lax.rem(x + NX - 1, NX), lax.rem(x + 2, NX)

    loads = []

    def load(src, dst):
        copy = pltpu.make_async_copy(src, dst, lsem.at[len(loads)])
        copy.start()
        loads.append(copy)
        return copy

    ld_tok = load(tok_h, tok)
    ld_ing = load(ing_h, ing)
    ld_dd = load(dd_h, dd)
    ld_du = load(du_h.at[:, pl.ds(pl.multiple_of(me * QUERY_FEATURES, QUERY_FEATURES), QUERY_FEATURES)], du)
    ld_off = load(off_h, doff)
    ld_ext = load(ext_h, ext)
    ld_wk = load(wk_h, wk)
    ld_wv = load(wv_h, wv)
    ld_wq = load(wq_h, wq)
    ld_wg = load(wg_h, wg)
    ld_hg = load(hg_h, hg)
    ld_wo = load(wo_h, wo)
    ld_og = load(og_h, og)

    barrier = pltpu.get_barrier_semaphore()
    peers = [{"y": lax.rem(y + o, ny)} for o in range(1, ny)]
    peers += [{"z": lax.rem(z + o, nz)} for o in range(1, nz)]
    tps = [(o, t) for o in range(NX) for t in range(2) if (o, t) != (0, 0)]
    tp_peers = [{"x": lax.rem(x + o, NX), "c": lax.rem(c + t, 2)} for o, t in tps]
    peers += tp_peers
    for peer in peers:
        pl.semaphore_signal(barrier, inc=1, device_id=peer, device_id_type=MESH)

    ld_tok.wait()
    ld_ing.wait()

    def norm_rows(i, carry):
        at = pl.ds(pl.multiple_of(i * 16, 16), 16)
        wide = tok[at, :].astype(f32)
        scale = lax.rsqrt(jnp.mean(wide * wide, axis=1, keepdims=True) + norm_eps)
        nrm[at, :] = (wide * scale * ing[...]).astype(bf16)
        return carry

    lax.fori_loop(0, rows // 16, norm_rows, 0, unroll=4)

    ld_dd.wait()
    ld_du.wait()
    ld_off.wait()
    ld_ext.wait()
    low = dot(nrm[...], dd[...]).astype(bf16)
    pre = dot(low, du[...]) + doff[...]
    log_decay = (jnp.minimum(pre, 0.0) - jnp.log1p(jnp.exp(-jnp.abs(pre)))) / decay_temper + ext[...]
    d_hi = log_decay.astype(bf16)
    rest = log_decay - d_hi.astype(f32)
    d_mid = rest.astype(bf16)
    d_low = (rest - d_mid.astype(f32)).astype(bf16)
    lower = lax.broadcasted_iota(jnp.int32, (rows, rows), 0) >= lax.broadcasted_iota(jnp.int32, (rows, rows), 1)
    lower = jnp.where(lower, 1.0, 0.0).astype(bf16)
    cum[...] = dot(lower, d_hi) + (dot(lower, d_mid) + dot(lower, d_low))
    closing = cum[rows - 1 : rows, :]
    gsend[...] = closing
    garr[y] = closing

    ld_wk.wait()
    ld_wv.wait()
    kk[...] = dot(nrm[...], wk[...]).astype(bf16)
    vv[...] = dot(nrm[...], wv[...]).astype(bf16)
    khat = (kk[...].astype(f32) * jnp.exp(closing - cum[...])).astype(bf16)
    state = dot(vv[...], khat, 0, 0).astype(bf16)
    st[...] = state.reshape(ny, piece, QUERY_FEATURES)
    arr[y] = st[y]

    pl.semaphore_wait(barrier, len(peers))

    def copy1(o):
        to = lax.rem(y + o, ny)
        return (
            pltpu.make_async_remote_copy(
                src_ref=st.at[to], dst_ref=arr.at[y], send_sem=s1s.at[o], recv_sem=s1r.at[o],
                device_id={"y": to}, device_id_type=MESH),
            pltpu.make_async_remote_copy(
                src_ref=gsend, dst_ref=garr.at[y], send_sem=g1s.at[o], recv_sem=g1r.at[o],
                device_id={"y": to}, device_id_type=MESH),
        )

    def got1(o):
        src = lax.rem(y + ny - o, ny)
        return (
            pltpu.make_async_remote_copy(
                src_ref=st.at[src], dst_ref=arr.at[src], send_sem=s1s.at[o], recv_sem=s1r.at[o],
                device_id={"y": src}, device_id_type=MESH),
            pltpu.make_async_remote_copy(
                src_ref=gsend, dst_ref=garr.at[src], send_sem=g1s.at[o], recv_sem=g1r.at[o],
                device_id={"y": src}, device_id_type=MESH),
        )

    for o in far_first(ny):
        for copy in copy1(o):
            copy.start()

    ld_wq.wait()
    qq[...] = dot(nrm[...], wq[...]).astype(bf16)
    qhat[...] = (qq[...].astype(f32) * jnp.exp(cum[...])).astype(bf16)
    ld_wg.wait()
    ld_hg.wait()
    gate = dot(nrm[...], wg[...]).astype(bf16).astype(f32)
    fac[...] = gate * (1.0 / (1.0 + jnp.exp(-gate))) * hg[...]

    for o in range(1, ny):
        for copy in got1(o):
            copy.wait_recv()
    run = jnp.zeros((piece, QUERY_FEATURES), f32)
    total = jnp.zeros((1, QUERY_FEATURES), f32)
    for k in range(ny):
        inside[k] = run
        wbuf[k] = jnp.exp(total)
        run = jnp.exp(garr[k]) * run + arr[k].astype(f32)
        total = total + garr[k]
    tsend[...] = run.astype(bf16)
    gtsend[...] = total

    def copy2(d):
        to = lax.rem(z + d, nz)
        return (
            pltpu.make_async_remote_copy(
                src_ref=tsend, dst_ref=zarr.at[d], send_sem=s2s.at[d], recv_sem=s2r.at[d],
                device_id={"z": to}, device_id_type=MESH),
            pltpu.make_async_remote_copy(
                src_ref=gtsend, dst_ref=zgarr.at[d], send_sem=g2s.at[d], recv_sem=g2r.at[d],
                device_id={"z": to}, device_id_type=MESH),
        )

    later = nz - 1 - z

    def send2(i, carry):
        for copy in copy2(later - i):
            copy.start()
        return carry

    lax.fori_loop(0, later, send2, 0)

    size = (CHUNK, CHUNK)
    r_at, c_at = lax.broadcasted_iota(jnp.int32, size, 0), lax.broadcasted_iota(jnp.int32, size, 1)
    mid = CHUNK // 2
    same = (r_at >= c_at) & ((r_at >= mid) == (c_at >= mid))
    cross = (r_at >= mid) & (c_at < mid)
    for i in range(chunks):
        lo = i * CHUNK
        own = slice(lo, lo + CHUNK)
        q = qq[own, :].astype(f32)
        k = kk[own, :].astype(f32)
        at = cum[own, :]
        pivot = jnp.concatenate(
            [jnp.broadcast_to(cum[lo + j + mid // 2 - 1 : lo + j + mid // 2, :], (mid, QUERY_FEATURES)) for j in (0, mid)], axis=0)
        border = cum[lo + mid - 1 : lo + mid, :]
        near = dot_wide(q * jnp.exp(at - pivot), k * jnp.exp(pivot - at))
        step = dot_wide(q * jnp.exp(jnp.minimum(at - border, 0.0)), k * jnp.exp(jnp.minimum(border - at, 0.0)))
        scores = jnp.where(same, near, jnp.where(cross, step, 0.0)).astype(bf16)
        result = dot(scores, vv[own, :])
        if i:
            start = cum[lo - 1 : lo, :]
            before = slice(0, lo)
            earlier = dot_wide(
                q * jnp.exp(at - start), kk[before, :].astype(f32) * jnp.exp(start - cum[before, :]))
            result = result + dot(earlier.astype(bf16), vv[before, :])
        att[own, :] = result

    def take2(d, carry):
        into, weight = carry
        for copy in copy2(d):
            copy.wait_recv()
        return into + jnp.exp(weight) * zarr[d].astype(f32), weight + zgarr[d]

    ahead, _ = lax.fori_loop(
        1, z + 1, take2,
        (jnp.zeros((piece, QUERY_FEATURES), f32), jnp.zeros((1, QUERY_FEATURES), f32)))

    for k in range(ny):
        bsend[k] = (wbuf[k] * ahead + inside[k]).astype(bf16)

    def copy3(o):
        to = lax.rem(y + o, ny)
        return pltpu.make_async_remote_copy(
            src_ref=bsend.at[to], dst_ref=sin.at[y], send_sem=s3s.at[o], recv_sem=s3r.at[o],
            device_id={"y": to}, device_id_type=MESH)

    def got3(o):
        src = lax.rem(y + ny - o, ny)
        return pltpu.make_async_remote_copy(
            src_ref=bsend.at[src], dst_ref=sin.at[src], send_sem=s3s.at[o], recv_sem=s3r.at[o],
            device_id={"y": src}, device_id_type=MESH)

    for o in far_first(ny):
        copy3(o).start()
    sin[y] = bsend[y]
    for o in range(1, ny):
        got3(o).wait_recv()
    come = sin[...].reshape(DV, QUERY_FEATURES)

    first, second = pl.ds(0, half), pl.ds(half, half)

    def go(slot, part, k, where):
        return pltpu.make_async_remote_copy(
            src_ref=gat.at[slot, part], dst_ref=gat.at[slot, part], send_sem=gs.at[k], recv_sem=gr.at[k],
            device_id=where, device_id_type=MESH)

    east, west, other = {"x": plus}, {"x": minus}, {"c": 1 - c}
    from_west, from_east, from_far = minus * 2 + c, plus * 2 + c, across * 2 + c
    twin = 1 - 2 * c

    for part, sends in ((first, ((0, east), (3, west), (6, other))), (second, ((2, west), (1, east), (7, other)))):
        there = att[part, :] + dot(qhat[part, :], come, 1, 1)
        scale = lax.rsqrt(jnp.mean(there * there, axis=1, keepdims=True) + norm_eps)
        gat[me, part, :] = (there * scale * fac[part, :]).astype(bf16)
        for k, where in sends:
            go(me, part, k, where).start()

    ld_wo.wait()

    def add(slot, part, fresh=False):
        term = dot(gat[slot, part, :], wo[pl.ds(pl.multiple_of(slot * DV, DV), DV), :])
        acc[part, :] = term if fresh else acc[part, :] + term

    add(me, first, True)
    add(me, second, True)
    go(from_west, first, 0, west).wait_recv()
    go(from_west, first, 4, east).start()
    go(from_west, first, 8, other).start()
    go(from_east, second, 2, east).wait_recv()
    go(from_east, second, 5, west).start()
    go(from_east, second, 9, other).start()
    go(me + twin, first, 6, other).wait_recv()
    go(me + twin, second, 7, other).wait_recv()
    add(me + twin, first)
    add(me + twin, second)
    add(from_west, first)
    add(from_east, second)
    go(from_west, second, 1, west).wait_recv()
    go(from_west, second, 10, other).start()
    go(from_east, first, 3, east).wait_recv()
    go(from_east, first, 11, other).start()
    add(from_west, second)
    add(from_east, first)
    go(from_west + twin, first, 8, other).wait_recv()
    add(from_west + twin, first)
    go(from_east + twin, second, 9, other).wait_recv()
    add(from_east + twin, second)
    go(from_west + twin, second, 10, other).wait_recv()
    add(from_west + twin, second)
    go(from_east + twin, first, 11, other).wait_recv()
    add(from_east + twin, first)
    go(from_far, first, 4, west).wait_recv()
    go(from_far, first, 12, other).start()
    go(from_far, second, 5, east).wait_recv()
    go(from_far, second, 13, other).start()
    add(from_far, first)
    add(from_far, second)
    go(from_far + twin, first, 12, other).wait_recv()
    add(from_far + twin, first)
    go(from_far + twin, second, 13, other).wait_recv()
    add(from_far + twin, second)

    mixed = acc[...]
    folded = mixed * mixed
    folded = folded[:, :128] + folded[:, 128:]
    ssend[...] = jnp.zeros_like(ssend)
    for i in range(chunks):
        flipped = folded[i * CHUNK : (i + 1) * CHUNK, :].T
        ssend[i : i + 1, :] = jnp.sum(flipped, axis=0, keepdims=True)

    def copy_ss(j):
        return pltpu.make_async_remote_copy(
            src_ref=ssend, dst_ref=sarr.at[me], send_sem=nss.at[j], recv_sem=nsr.at[j],
            device_id=tp_peers[j], device_id_type=MESH)

    def got_ss(j):
        o, t = tps[j]
        src_x, src_c = lax.rem(x + NX - o, NX), lax.rem(c + t, 2)
        return pltpu.make_async_remote_copy(
            src_ref=ssend, dst_ref=sarr.at[src_x * 2 + src_c], send_sem=nss.at[j], recv_sem=nsr.at[j],
            device_id={"x": src_x, "c": src_c}, device_id_type=MESH)

    for j in range(len(tps)):
        copy_ss(j).start()
    sarr[me] = ssend[...]
    ld_og.wait()
    for j in range(len(tps)):
        got_ss(j).wait_recv()
    squares = sarr[0]
    for j in range(1, 2 * NX):
        squares = squares + sarr[j]
    inverse = lax.rsqrt(squares / (2 * NX * DV) + norm_eps)
    for i in range(chunks):
        own = slice(i * CHUNK, (i + 1) * CHUNK)
        per_row = jnp.broadcast_to(inverse[i : i + 1, :], size).T
        for j in range(0, DV, 128):
            out_ref[own, j : j + 128] = (acc[own, j : j + 128] * per_row * og[:, j : j + 128]).astype(out_ref.dtype)

    for o in range(1, ny):
        for copy in copy1(o):
            copy.wait_send()
        copy3(o).wait_send()

    def sent2(i, carry):
        for copy in copy2(later - i):
            copy.wait_send()
        return carry

    lax.fori_loop(0, later, sent2, 0)
    for k, part in enumerate((first, second, second, first, first, second, first, second,
                              first, second, second, first, first, second)):
        go(me, part, k, other).wait_send()
    for j in range(len(tps)):
        copy_ss(j).wait_send()


def local(nz, ny, *args):
    (tokens, in_gain, query_weight, key_weight, value_weight, gate_weight, decay_down, decay_up,
     decay_offset, decay_extra, head_gain, out_weight, out_gain) = args
    rows, width = tokens.shape
    piece = DV // ny
    rank = decay_down.shape[1]
    in_hbm = pl.BlockSpec(memory_space=pltpu.HBM)
    dma = pltpu.SemaphoreType.DMA
    V = pltpu.VMEM
    scratch = [
        V((rows, width), bf16),
        V((rows, width), bf16),
        V((width, QUERY_FEATURES), bf16),
        V((width, QUERY_FEATURES), bf16),
        V((width, DV), bf16),
        V((width, DV), bf16),
        V((2 * NX * DV, DV), bf16),
        V((width, rank), bf16),
        V((rank, QUERY_FEATURES), bf16),
        V((1, width), f32),
        V((1, QUERY_FEATURES), f32),
        V((rows, QUERY_FEATURES), f32),
        V((1, DV), f32),
        V((1, DV), f32),
        V((rows, QUERY_FEATURES), f32),
        V((rows, QUERY_FEATURES), bf16),
        V((rows, DV), bf16),
        V((rows, QUERY_FEATURES), bf16),
        V((rows, DV), f32),
        V((rows, QUERY_FEATURES), bf16),
        V((rows, DV), f32),
        V((ny, piece, QUERY_FEATURES), bf16),
        V((1, QUERY_FEATURES), f32),
        V((ny, piece, QUERY_FEATURES), bf16),
        V((ny, 1, QUERY_FEATURES), f32),
        V((ny, piece, QUERY_FEATURES), f32),
        V((ny, 1, QUERY_FEATURES), f32),
        V((piece, QUERY_FEATURES), bf16),
        V((1, QUERY_FEATURES), f32),
        V((nz, piece, QUERY_FEATURES), bf16),
        V((nz, 1, QUERY_FEATURES), f32),
        V((ny, piece, QUERY_FEATURES), bf16),
        V((ny, piece, QUERY_FEATURES), bf16),
        V((2 * NX, rows, DV), bf16),
        V((rows, DV), f32),
        V((8, 128), f32),
        V((2 * NX, 8, 128), f32),
        dma((13,)),
        dma((ny,)), dma((ny,)), dma((ny,)), dma((ny,)),
        dma((nz,)), dma((nz,)), dma((nz,)), dma((nz,)),
        dma((ny,)), dma((ny,)),
        dma((14,)), dma((14,)),
        dma((2 * NX - 1,)), dma((2 * NX - 1,)),
    ]
    return pl.pallas_call(
        functools.partial(kernel, nz, ny),
        out_shape=jax.ShapeDtypeStruct((rows, DV), bf16),
        in_specs=[in_hbm] * 13,
        out_specs=pl.BlockSpec(memory_space=pltpu.VMEM),
        scratch_shapes=scratch,
        compiler_params=pltpu.CompilerParams(collective_id=0, has_side_effects=True, vmem_limit_bytes=48 << 20),
        name="linear_attention",
    )(
        tokens, in_gain.reshape(1, -1), query_weight, key_weight, value_weight, gate_weight, decay_down, decay_up,
        decay_offset.reshape(1, -1), decay_extra, head_gain.reshape(1, -1), out_weight, out_gain.reshape(1, -1),
    )


def build(devices, nz, ny):
    torus = Mesh(devices.reshape(nz, ny, NX, 2), ("z", "y", "x", "c"))
    sp, tp = ("z", "y"), ("x", "c")
    in_specs = (
        P(sp, None), P(), P(None, tp), P(None, tp), P(None, tp), P(None, tp), P(), P(), P(tp),
        P(sp, tp), P(tp), P(None, tp), P(tp),
    )
    return jax.shard_map(
        functools.partial(local, nz, ny), mesh=torus, in_specs=in_specs, out_specs=P(sp, tp), check_vma=False)


def solution(mesh):
    ny = 8
    return build(mesh.devices, mesh.shape["sp"] // ny, ny)
```

time: 218 us -> 61.4 us (0.28)
  the two profiles are of different devices: /device:TPU:1 before, /device:TPU:65 now
where the time goes in v1:
time: 61.4 us; the launch traced here: 60.8 us
  Pallas kernels  48.7 us (79%)
  local copies, waits for them, and re-layouts  12.1 us (20%)
    pallas_call x1, Pallas kernels, local(): pl.pallas_call(functools.partial(kernel, nz, ny), out_shape=jax.ShapeDtyp...  48.7 us
    unnamed x24, local copies, waits for them, and re-layouts  12.1 us

profile of v1, /device:TPU:65, one launch (start us, length us, event | category | flops | bytes accessed | tf_op | source)
XLA Modules:
  0.0 60.8 jit_solution(721911713880139729)
XLA Ops:
  0.0 1.2 %copy.14.dd_h = bf16[2048,32]{1,0:T(8,128)(2,1)S(1)} copy(bf16[2048,32]{0,1:T(8,128)(2,1)} %param.19) | data formatting | bytes 262144 | tf_op args[6]
  1.2 0.0 copy-start
  1.2 1.2 %copy-done = bf16[2048,256]{1,0:T(8,128)(2,1)S(1)} copy-done((bf16[2048,256]{1,0:T(8,128)(2,1)S(1)}, bf16[2048,256]{1,0:T(8,128)(2,1)}, u32[]{:S(2)}) %copy-start) | copy-done | bytes 1048600
  2.4 0.0 copy-start.1
  2.4 1.2 %copy-done.1 = bf16[2048,256]{1,0:T(8,128)(2,1)S(1)} copy-done((bf16[2048,256]{1,0:T(8,128)(2,1)S(1)}, bf16[2048,256]{1,0:T(8,128)(2,1)}, u32[]{:S(2)}) %copy-start.1) | copy-done | bytes 1048600
  3.6 0.0 copy-start.2
  3.6 1.2 %copy-done.2 = bf16[2048,256]{1,0:T(8,128)(2,1)S(1)} copy-done((bf16[2048,256]{1,0:T(8,128)(2,1)S(1)}, bf16[2048,256]{1,0:T(8,128)(2,1)}, u32[]{:S(2)}) %copy-start.2) | copy-done | bytes 1048600
  4.9 0.0 copy-start.3
  4.9 1.0 %copy-done.3 = bf16[2048,128]{1,0:T(8,128)(2,1)S(1)} copy-done((bf16[2048,128]{1,0:T(8,128)(2,1)S(1)}, bf16[2048,128]{1,0:T(8,128)(2,1)}, u32[]{:S(2)}) %copy-start.3) | copy-done | bytes 524312
  5.9 0.0 copy-start.4
  5.9 1.0 %copy-done.4 = bf16[2048,128]{1,0:T(8,128)(2,1)S(1)} copy-done((bf16[2048,128]{1,0:T(8,128)(2,1)S(1)}, bf16[2048,128]{1,0:T(8,128)(2,1)}, u32[]{:S(2)}) %copy-start.4) | copy-done | bytes 524312
  6.9 0.0 copy-start.5
  6.9 0.9 %copy-done.5 = f32[384,128]{1,0:T(8,128)S(1)} copy-done((f32[384,128]{1,0:T(8,128)S(1)}, f32[384,128]{1,0:T(8,128)}, u32[]{:S(2)}) %copy-start.5) | copy-done | bytes 196632
  7.9 0.0 copy-start.6
  7.9 0.8 %copy-done.6 = bf16[32,1024]{1,0:T(8,128)(2,1)S(1)} copy-done((bf16[32,1024]{1,0:T(8,128)(2,1)S(1)}, bf16[32,1024]{1,0:T(8,128)(2,1)}, u32[]{:S(2)}) %copy-start.6) | copy-done | bytes 65560
  8.7 0.0 copy-start.7
  8.7 0.7 %copy-done.7 = f32[2048]{0:T(1024)S(1)} copy-done((f32[2048]{0:T(1024)S(1)}, f32[2048]{0:T(1024)}, u32[]{:S(2)}) %copy-start.7) | copy-done | bytes 8216
  9.4 0.0 copy-start.8
  9.4 0.7 %copy-done.8 = f32[256]{0:T(256)S(1)} copy-done((f32[256]{0:T(256)S(1)}, f32[256]{0:T(256)}, u32[]{:S(2)}) %copy-start.8) | copy-done | bytes 1048
  10.1 0.0 copy-start.9
  10.1 0.7 %copy-done.9 = f32[256]{0:T(256)S(1)} copy-done((f32[256]{0:T(256)S(1)}, f32[256]{0:T(256)}, u32[]{:S(2)}) %copy-start.9) | copy-done | bytes 1048
  10.8 0.7 %copy-done.10 = f32[128]{0:T(128)S(1)} copy-done((f32[128]{0:T(128)S(1)}, f32[128]{0:T(128)}, u32[]{:S(2)}) %copy-start.10) | copy-done | bytes 536
  11.4 48.7 %linear_attention.1 = bf16[384,256]{1,0:T(8,128)(2,1)S(1)} custom-call(bf16[384,2048]{1,0:T(8,128)(2,1)} %tok_h.1, f32[1,2048]{1,0:T(1,128)S(1)} %bitcast.4, bf16[2048,128]{1,0:T(8,128)(2,1)S(1)} %copy-done.3, bf16[2048,128]{1,0:T(8,128)(2,1)S(1)} %copy-done.4, bf16[2048,256]{1,0:T(8,128)(2,1)S(1)} %copy-done, bf16[2048,256]{1,0:T(8,128)(2,1)S(1)} %copy-done.1, ...), custom_call_target="tpu_custom_call" | custom-call | tf_op jit(solution)/shard_map/linear_attention/pallas_call | solution.py:482
  60.2 0.7 %copy.16 = bf16[384,256]{1,0:T(8,128)(2,1)} copy(bf16[384,256]{1,0:T(8,128)(2,1)S(1)} %linear_attention.1) | data formatting | bytes 393216
  (1 shorter events, 0.0 us)
Async XLA Ops:
  1.2 1.2 %copy-start = (bf16[2048,256]{1,0:T(8,128)(2,1)S(1)}, bf16[2048,256]{1,0:T(8,128)(2,1)}, u32[]{:S(2)}) copy-start(bf16[2048,256]{1,0:T(8,128)(2,1)} %wv_h.1) | copy-start | bytes 3145732
  2.4 1.2 %copy-start.1 = (bf16[2048,256]{1,0:T(8,128)(2,1)S(1)}, bf16[2048,256]{1,0:T(8,128)(2,1)}, u32[]{:S(2)}) copy-start(bf16[2048,256]{1,0:T(8,128)(2,1)} %wg_h.1) | copy-start | bytes 3145732
  3.6 1.2 %copy-start.2 = (bf16[2048,256]{1,0:T(8,128)(2,1)S(1)}, bf16[2048,256]{1,0:T(8,128)(2,1)}, u32[]{:S(2)}) copy-start(bf16[2048,256]{1,0:T(8,128)(2,1)} %wo_h.1) | copy-start | bytes 3145732
  4.9 1.0 %copy-start.3 = (bf16[2048,128]{1,0:T(8,128)(2,1)S(1)}, bf16[2048,128]{1,0:T(8,128)(2,1)}, u32[]{:S(2)}) copy-start(bf16[2048,128]{1,0:T(8,128)(2,1)} %wq_h.1) | copy-start | bytes 1572868
  5.9 1.0 %copy-start.4 = (bf16[2048,128]{1,0:T(8,128)(2,1)S(1)}, bf16[2048,128]{1,0:T(8,128)(2,1)}, u32[]{:S(2)}) copy-start(bf16[2048,128]{1,0:T(8,128)(2,1)} %wk_h.1) | copy-start | bytes 1572868
  6.9 0.9 %copy-start.5 = (f32[384,128]{1,0:T(8,128)S(1)}, f32[384,128]{1,0:T(8,128)}, u32[]{:S(2)}) copy-start(f32[384,128]{1,0:T(8,128)} %ext_h.1) | copy-start | bytes 589828
  7.9 0.8 %copy-start.6 = (bf16[32,1024]{1,0:T(8,128)(2,1)S(1)}, bf16[32,1024]{1,0:T(8,128)(2,1)}, u32[]{:S(2)}) copy-start(bf16[32,1024]{1,0:T(8,128)(2,1)} %du_h.1) | copy-start | bytes 196612
  8.7 0.7 %copy-start.7 = (f32[2048]{0:T(1024)S(1)}, f32[2048]{0:T(1024)}, u32[]{:S(2)}) copy-start(f32[2048]{0:T(1024)} %param.14) | copy-start | bytes 24580
  9.4 0.7 %copy-start.8 = (f32[256]{0:T(256)S(1)}, f32[256]{0:T(256)}, u32[]{:S(2)}) copy-start(f32[256]{0:T(256)} %param.23) | copy-start | bytes 3076
  10.1 0.7 %copy-start.9 = (f32[256]{0:T(256)S(1)}, f32[256]{0:T(256)}, u32[]{:S(2)}) copy-start(f32[256]{0:T(256)} %param.25) | copy-start | bytes 3076
  10.8 0.7 %copy-start.10 = (f32[128]{0:T(128)S(1)}, f32[128]{0:T(128)}, u32[]{:S(2)}) copy-start(f32[128]{0:T(128)} %param.21) | copy-start | bytes 1540

commit v2 on v1

--- a/solution.py
+++ b/solution.py
@@ -11,6 +11,8 @@
 QUERY_FEATURES = 128
 DV = 256
 CHUNK = 128
+TOKEN_PARTS = 4
+GROUP = 4
 NX = 4
 norm_eps = 1e-06
 decay_temper = 16.0
@@ -81,12 +83,15 @@
     gtsend,
     zarr,
     zgarr,
+    zfar,
+    zgfar,
     bsend,
     sin,
     gat,
     acc,
     ssend,
     sarr,
+    ready,
     lsem,
     s1s,
     s1r,
@@ -96,6 +101,8 @@
     s2r,
     g2s,
     g2r,
+    s2f,
+    g2f,
     s3s,
     s3r,
     gs,
@@ -119,8 +126,9 @@
         loads.append(copy)
         return copy
 
-    ld_tok = load(tok_h, tok)
     ld_ing = load(ing_h, ing)
+    part_rows = rows // TOKEN_PARTS
+    ld_tok = [load(tok_h.at[pl.ds(i * part_rows, part_rows)], tok.at[pl.ds(i * part_rows, part_rows)]) for i in range(TOKEN_PARTS)]
     ld_dd = load(dd_h, dd)
     ld_du = load(du_h.at[:, pl.ds(pl.multiple_of(me * QUERY_FEATURES, QUERY_FEATURES), QUERY_FEATURES)], du)
     ld_off = load(off_h, doff)
@@ -135,14 +143,22 @@
 
     barrier = pltpu.get_barrier_semaphore()
     peers = [{"y": lax.rem(y + o, ny)} for o in range(1, ny)]
-    peers += [{"z": lax.rem(z + o, nz)} for o in range(1, nz)]
     tps = [(o, t) for o in range(NX) for t in range(2) if (o, t) != (0, 0)]
     tp_peers = [{"x": lax.rem(x + o, NX), "c": lax.rem(c + t, 2)} for o, t in tps]
     peers += tp_peers
     for peer in peers:
         pl.semaphore_signal(barrier, inc=1, device_id=peer, device_id_type=MESH)
-
-    ld_tok.wait()
+    later = nz - 1 - z
+    group, place = lax.div(z, GROUP), lax.rem(z, GROUP)
+    last = place == GROUP - 1
+    reach = jnp.where(last, later, GROUP - 1 - place)
+
+    def greet(d, carry):
+        pl.semaphore_signal(barrier, inc=1, device_id={"z": z + d}, device_id_type=MESH)
+        return carry
+
+    lax.fori_loop(1, reach + 1, greet, 0)
+
     ld_ing.wait()
 
     def norm_rows(i, carry):
@@ -152,13 +168,18 @@
         nrm[at, :] = (wide * scale * ing[...]).astype(bf16)
         return carry
 
-    lax.fori_loop(0, rows // 16, norm_rows, 0, unroll=4)
+    tiles = part_rows // 16
+    for i in range(TOKEN_PARTS):
+        ld_tok[i].wait()
+        lax.fori_loop(i * tiles, (i + 1) * tiles, norm_rows, 0, unroll=3)
 
     ld_dd.wait()
     ld_du.wait()
     ld_off.wait()
     ld_ext.wait()
-    low = dot(nrm[...], dd[...]).astype(bf16)
+    ld_wk.wait()
+    ld_wv.wait()
+    low = dot(nrm[...], dd[...], 1, 1).astype(bf16)
     pre = dot(low, du[...]) + doff[...]
     log_decay = (jnp.minimum(pre, 0.0) - jnp.log1p(jnp.exp(-jnp.abs(pre)))) / decay_temper + ext[...]
     d_hi = log_decay.astype(bf16)
@@ -172,8 +193,6 @@
     gsend[...] = closing
     garr[y] = closing
 
-    ld_wk.wait()
-    ld_wv.wait()
     kk[...] = dot(nrm[...], wk[...]).astype(bf16)
     vv[...] = dot(nrm[...], wv[...]).astype(bf16)
     khat = (kk[...].astype(f32) * jnp.exp(closing - cum[...])).astype(bf16)
@@ -181,33 +200,36 @@
     st[...] = state.reshape(ny, piece, QUERY_FEATURES)
     arr[y] = st[y]
 
-    pl.semaphore_wait(barrier, len(peers))
-
     def copy1(o):
         to = lax.rem(y + o, ny)
         return (
             pltpu.make_async_remote_copy(
-                src_ref=st.at[to], dst_ref=arr.at[y], send_sem=s1s.at[o], recv_sem=s1r.at[o],
+                src_ref=st.at[to], dst_ref=arr.at[y], send_sem=s1s, recv_sem=s1r,
                 device_id={"y": to}, device_id_type=MESH),
             pltpu.make_async_remote_copy(
-                src_ref=gsend, dst_ref=garr.at[y], send_sem=g1s.at[o], recv_sem=g1r.at[o],
+                src_ref=gsend, dst_ref=garr.at[y], send_sem=g1s, recv_sem=g1r,
                 device_id={"y": to}, device_id_type=MESH),
         )
 
-    def got1(o):
-        src = lax.rem(y + ny - o, ny)
-        return (
-            pltpu.make_async_remote_copy(
-                src_ref=st.at[src], dst_ref=arr.at[src], send_sem=s1s.at[o], recv_sem=s1r.at[o],
-                device_id={"y": src}, device_id_type=MESH),
-            pltpu.make_async_remote_copy(
-                src_ref=gsend, dst_ref=garr.at[src], send_sem=g1s.at[o], recv_sem=g1r.at[o],
-                device_id={"y": src}, device_id_type=MESH),
-        )
-
+    def all_of(ref, count, sem):
+        some = ref.at[pl.ds(0, count)]
+        pltpu.make_async_copy(some, some, sem).wait()
+
+    pl.semaphore_wait(barrier, len(peers) + place + group)
     for o in far_first(ny):
         for copy in copy1(o):
             copy.start()
+
+    def tell_near(d, carry):
+        pl.semaphore_signal(ready, inc=1, device_id={"z": z - d}, device_id_type=MESH)
+        return carry
+
+    def tell_last(g, carry):
+        pl.semaphore_signal(ready, inc=1, device_id={"z": g * GROUP + GROUP - 1}, device_id_type=MESH)
+        return carry
+
+    lax.fori_loop(1, place + 1, tell_near, 0)
+    lax.fori_loop(0, group, tell_last, 0)
 
     ld_wq.wait()
     qq[...] = dot(nrm[...], wq[...]).astype(bf16)
@@ -216,39 +238,6 @@
     ld_hg.wait()
     gate = dot(nrm[...], wg[...]).astype(bf16).astype(f32)
     fac[...] = gate * (1.0 / (1.0 + jnp.exp(-gate))) * hg[...]
-
-    for o in range(1, ny):
-        for copy in got1(o):
-            copy.wait_recv()
-    run = jnp.zeros((piece, QUERY_FEATURES), f32)
-    total = jnp.zeros((1, QUERY_FEATURES), f32)
-    for k in range(ny):
-        inside[k] = run
-        wbuf[k] = jnp.exp(total)
-        run = jnp.exp(garr[k]) * run + arr[k].astype(f32)
-        total = total + garr[k]
-    tsend[...] = run.astype(bf16)
-    gtsend[...] = total
-
-    def copy2(d):
-        to = lax.rem(z + d, nz)
-        return (
-            pltpu.make_async_remote_copy(
-                src_ref=tsend, dst_ref=zarr.at[d], send_sem=s2s.at[d], recv_sem=s2r.at[d],
-                device_id={"z": to}, device_id_type=MESH),
-            pltpu.make_async_remote_copy(
-                src_ref=gtsend, dst_ref=zgarr.at[d], send_sem=g2s.at[d], recv_sem=g2r.at[d],
-                device_id={"z": to}, device_id_type=MESH),
-        )
-
-    later = nz - 1 - z
-
-    def send2(i, carry):
-        for copy in copy2(later - i):
-            copy.start()
-        return carry
-
-    lax.fori_loop(0, later, send2, 0)
 
     size = (CHUNK, CHUNK)
     r_at, c_at = lax.broadcasted_iota(jnp.int32, size, 0), lax.broadcasted_iota(jnp.int32, size, 1)
@@ -276,55 +265,116 @@
             result = result + dot(earlier.astype(bf16), vv[before, :])
         att[own, :] = result
 
-    def take2(d, carry):
+    all_of(arr, ny - 1, s1r)
+    all_of(garr, ny - 1, g1r)
+    run = jnp.zeros((piece, QUERY_FEATURES), f32)
+    total = jnp.zeros((1, QUERY_FEATURES), f32)
+    for k in range(ny):
+        inside[k] = run
+        wbuf[k] = jnp.exp(total)
+        run = jnp.exp(garr[k]) * run + arr[k].astype(f32)
+        total = total + garr[k]
+    tsend[0] = run.astype(bf16)
+    gtsend[0] = total
+
+    def copy2(level, d, slot, recv):
+        send, land = (s2s, g2s), ((zarr, zgarr), (zfar, zgfar))[level]
+        to = {"z": lax.rem(z + d, nz)}
+        return [
+            pltpu.make_async_remote_copy(
+                src_ref=src.at[level], dst_ref=dst.at[slot], send_sem=sem.at[level], recv_sem=got.at[slot],
+                device_id=to, device_id_type=MESH)
+            for src, dst, sem, got in zip((tsend, gtsend), land, send, recv)
+        ]
+
+    @pl.when(reach > 0)
+    def _():
+        pl.semaphore_wait(ready, reach)
+
+    def send_near(i, carry):
+        d = GROUP - 1 - place - i
+        for copy in copy2(0, d, d, (s2r, g2r)):
+            copy.start()
+        return carry
+
+    lax.fori_loop(0, GROUP - 1 - place, send_near, 0)
+
+    def take_near(d, carry):
         into, weight = carry
-        for copy in copy2(d):
+        for copy in copy2(0, d, d, (s2r, g2r)):
             copy.wait_recv()
         return into + jnp.exp(weight) * zarr[d].astype(f32), weight + zgarr[d]
 
-    ahead, _ = lax.fori_loop(
-        1, z + 1, take2,
-        (jnp.zeros((piece, QUERY_FEATURES), f32), jnp.zeros((1, QUERY_FEATURES), f32)))
+    nothing = (jnp.zeros((piece, QUERY_FEATURES), f32), jnp.zeros((1, QUERY_FEATURES), f32))
+    near, near_weight = lax.fori_loop(1, place + 1, take_near, nothing)
+
+    @pl.when(last)
+    def _():
+        tsend[1] = (jnp.exp(total) * near + run).astype(bf16)
+        gtsend[1] = near_weight + total
+
+        def send_far(d, carry):
+            for copy in copy2(1, d, group, (s2f, g2f)):
+                copy.start()
+            return carry
+
+        lax.fori_loop(1, later + 1, send_far, 0)
+
+    def take_far(i, carry):
+        into, weight = carry
+        g = group - 1 - i
+        for copy in copy2(1, 1, g, (s2f, g2f)):
+            copy.wait_recv()
+        return into + jnp.exp(weight) * zfar[g].astype(f32), weight + zgfar[g]
+
+    far, _ = lax.fori_loop(0, group, take_far, nothing)
+    ahead = jnp.exp(near_weight) * far + near
 
     for k in range(ny):
         bsend[k] = (wbuf[k] * ahead + inside[k]).astype(bf16)
 
+    first_of_all = (z == 0) & (y == 0)
+
     def copy3(o):
         to = lax.rem(y + o, ny)
+        slot = y + jnp.where((z == 0) & (to == 0), ny, 0)
         return pltpu.make_async_remote_copy(
-            src_ref=bsend.at[to], dst_ref=sin.at[y], send_sem=s3s.at[o], recv_sem=s3r.at[o],
+            src_ref=bsend.at[to], dst_ref=sin.at[slot], send_sem=s3s, recv_sem=s3r,
             device_id={"y": to}, device_id_type=MESH)
-
-    def got3(o):
-        src = lax.rem(y + ny - o, ny)
-        return pltpu.make_async_remote_copy(
-            src_ref=bsend.at[src], dst_ref=sin.at[src], send_sem=s3s.at[o], recv_sem=s3r.at[o],
-            device_id={"y": src}, device_id_type=MESH)
 
     for o in far_first(ny):
         copy3(o).start()
-    sin[y] = bsend[y]
-    for o in range(1, ny):
-        got3(o).wait_recv()
-    come = sin[...].reshape(DV, QUERY_FEATURES)
+
+    @pl.when(first_of_all)
+    def _():
+        sin[pl.ds(0, ny)] = jnp.zeros((ny, piece, QUERY_FEATURES), bf16)
+
+    @pl.when(jnp.logical_not(first_of_all))
+    def _():
+        sin[y] = bsend[y]
+        all_of(sin, ny - 1, s3r)
+
+    come = sin[pl.ds(0, ny)].reshape(DV, QUERY_FEATURES)
 
     first, second = pl.ds(0, half), pl.ds(half, half)
 
     def go(slot, part, k, where):
         return pltpu.make_async_remote_copy(
-            src_ref=gat.at[slot, part], dst_ref=gat.at[slot, part], send_sem=gs.at[k], recv_sem=gr.at[k],
+            src_ref=gat.at[slot, part], dst_ref=gat.at[slot, part], send_sem=gs, recv_sem=gr.at[k],
             device_id=where, device_id_type=MESH)
 
     east, west, other = {"x": plus}, {"x": minus}, {"c": 1 - c}
     from_west, from_east, from_far = minus * 2 + c, plus * 2 + c, across * 2 + c
     twin = 1 - 2 * c
 
-    for part, sends in ((first, ((0, east), (3, west), (6, other))), (second, ((2, west), (1, east), (7, other)))):
+    for part, sends in ((first, ((0, east), (6, other))), (second, ((2, west), (7, other)))):
         there = att[part, :] + dot(qhat[part, :], come, 1, 1)
         scale = lax.rsqrt(jnp.mean(there * there, axis=1, keepdims=True) + norm_eps)
         gat[me, part, :] = (there * scale * fac[part, :]).astype(bf16)
         for k, where in sends:
             go(me, part, k, where).start()
+    go(me, second, 1, east).start()
+    go(me, first, 3, west).start()
 
     ld_wo.wait()
 
@@ -381,22 +431,14 @@
 
     def copy_ss(j):
         return pltpu.make_async_remote_copy(
-            src_ref=ssend, dst_ref=sarr.at[me], send_sem=nss.at[j], recv_sem=nsr.at[j],
+            src_ref=ssend, dst_ref=sarr.at[me], send_sem=nss, recv_sem=nsr,
             device_id=tp_peers[j], device_id_type=MESH)
-
-    def got_ss(j):
-        o, t = tps[j]
-        src_x, src_c = lax.rem(x + NX - o, NX), lax.rem(c + t, 2)
-        return pltpu.make_async_remote_copy(
-            src_ref=ssend, dst_ref=sarr.at[src_x * 2 + src_c], send_sem=nss.at[j], recv_sem=nsr.at[j],
-            device_id={"x": src_x, "c": src_c}, device_id_type=MESH)
 
     for j in range(len(tps)):
         copy_ss(j).start()
     sarr[me] = ssend[...]
     ld_og.wait()
-    for j in range(len(tps)):
-        got_ss(j).wait_recv()
+    all_of(sarr, len(tps), nsr)
     squares = sarr[0]
     for j in range(1, 2 * NX):
         squares = squares + sarr[j]
@@ -407,22 +449,28 @@
         for j in range(0, DV, 128):
             out_ref[own, j : j + 128] = (acc[own, j : j + 128] * per_row * og[:, j : j + 128]).astype(out_ref.dtype)
 
-    for o in range(1, ny):
-        for copy in copy1(o):
-            copy.wait_send()
-        copy3(o).wait_send()
-
-    def sent2(i, carry):
-        for copy in copy2(later - i):
-            copy.wait_send()
-        return carry
-
-    lax.fori_loop(0, later, sent2, 0)
-    for k, part in enumerate((first, second, second, first, first, second, first, second,
-                              first, second, second, first, first, second)):
-        go(me, part, k, other).wait_send()
-    for j in range(len(tps)):
-        copy_ss(j).wait_send()
+    @pl.when(first_of_all)
+    def _():
+        all_of(sin, ny - 1, s3r)
+
+    all_of(st, ny - 1, s1s)
+    all_of(garr, ny - 1, g1s)
+    all_of(bsend, ny - 1, s3s)
+    all_of(sarr, len(tps), nss)
+
+    for p in range(GROUP - 1):
+        @pl.when(place == p)
+        def _(count=GROUP - 1 - p):
+            all_of(zfar, count, s2s.at[0])
+            all_of(zgfar, count, g2s.at[0])
+
+    for g in range(nz // GROUP - 1):
+        @pl.when(last & (group == g))
+        def _(count=nz - GROUP * (g + 1)):
+            all_of(zfar, count, s2s.at[1])
+            all_of(zgfar, count, g2s.at[1])
+
+    all_of(gat, 7, gs)
 
 
 def local(nz, ny, *args):
@@ -442,7 +490,7 @@
         V((width, DV), bf16),
         V((width, DV), bf16),
         V((2 * NX * DV, DV), bf16),
-        V((width, rank), bf16),
+        V((rank, width), bf16),
         V((rank, QUERY_FEATURES), bf16),
         V((1, width), f32),
         V((1, QUERY_FEATURES), f32),
@@ -462,23 +510,30 @@
         V((ny, 1, QUERY_FEATURES), f32),
         V((ny, piece, QUERY_FEATURES), f32),
         V((ny, 1, QUERY_FEATURES), f32),
-        V((piece, QUERY_FEATURES), bf16),
-        V((1, QUERY_FEATURES), f32),
+        V((2, piece, QUERY_FEATURES), bf16),
+        V((2, 1, QUERY_FEATURES), f32),
+        V((GROUP, piece, QUERY_FEATURES), bf16),
+        V((GROUP, 1, QUERY_FEATURES), f32),
         V((nz, piece, QUERY_FEATURES), bf16),
         V((nz, 1, QUERY_FEATURES), f32),
         V((ny, piece, QUERY_FEATURES), bf16),
-        V((ny, piece, QUERY_FEATURES), bf16),
+        V((2 * ny, piece, QUERY_FEATURES), bf16),
         V((2 * NX, rows, DV), bf16),
         V((rows, DV), f32),
         V((8, 128), f32),
         V((2 * NX, 8, 128), f32),
-        dma((13,)),
-        dma((ny,)), dma((ny,)), dma((ny,)), dma((ny,)),
-        dma((nz,)), dma((nz,)), dma((nz,)), dma((nz,)),
-        dma((ny,)), dma((ny,)),
-        dma((14,)), dma((14,)),
-        dma((2 * NX - 1,)), dma((2 * NX - 1,)),
+        pltpu.SemaphoreType.REGULAR,
+        dma((12 + TOKEN_PARTS,)),
+        dma, dma, dma, dma,
+        dma((2,)), dma((GROUP,)), dma((2,)), dma((GROUP,)), dma((nz // GROUP,)), dma((nz // GROUP,)),
+        dma, dma,
+        dma, dma((14,)),
+        dma, dma,
     ]
+    operands = (
+        tokens, in_gain.reshape(1, -1), query_weight, key_weight, value_weight, gate_weight, decay_down.T, decay_up,
+        decay_offset.reshape(1, -1), decay_extra, head_gain.reshape(1, -1), out_weight, out_gain.reshape(1, -1),
+    )
     return pl.pallas_call(
         functools.partial(kernel, nz, ny),
         out_shape=jax.ShapeDtypeStruct((rows, DV), bf16),
@@ -487,10 +542,7 @@
         scratch_shapes=scratch,
         compiler_params=pltpu.CompilerParams(collective_id=0, has_side_effects=True, vmem_limit_bytes=48 << 20),
         name="linear_attention",
-    )(
-        tokens, in_gain.reshape(1, -1), query_weight, key_weight, value_weight, gate_weight, decay_down, decay_up,
-        decay_offset.reshape(1, -1), decay_extra, head_gain.reshape(1, -1), out_weight, out_gain.reshape(1, -1),
-    )
+    )(*(pltpu.with_memory_space_constraint(operand, pltpu.HBM) for operand in operands))
 
 
 def build(devices, nz, ny):

time: 61.4 us -> 45.6 us (0.74)
  the two profiles are of different devices: /device:TPU:65 before, /device:TPU:256 now
where the time goes in v2:
time: 45.6 us; the launch traced here: 45.5 us
  Pallas kernels  44.8 us (98%)
  local copies, waits for them, and re-layouts  0.68 us (1%)
    pallas_call x1, Pallas kernels, local(): pl.pallas_call(functools.partial(kernel, nz, ny), out_shape=jax.ShapeDtyp...  44.8 us

profile of v2, /device:TPU:256, one launch (start us, length us, event | category | flops | bytes accessed | tf_op | source)
XLA Modules:
  0.0 45.5 jit_solution(17167993601317555182)
XLA Ops:
  0.0 44.8 %linear_attention.1 = bf16[384,256]{1,0:T(8,128)(2,1)S(1)} custom-call(bf16[384,2048]{1,0:T(8,128)(2,1)} %tok_h.1, f32[1,2048]{1,0:T(1,128)} %bitcast.6, bf16[2048,128]{1,0:T(8,128)(2,1)} %wq_h.1, bf16[2048,128]{1,0:T(8,128)(2,1)} %wk_h.1, bf16[2048,256]{1,0:T(8,128)(2,1)} %wv_h.1, bf16[2048,256]{1,0:T(8,128)(2,1)} %wg_h.1, bf16[32,2048]{1,0:T(8,128)(2,1)} %bitcast.5, ...), custom_call_target="tpu_custom_call" | custom-call | tf_op jit(solution)/shard_map/linear_attention/pallas_call | solution.py:537
  44.8 0.7 %copy.15 = bf16[384,256]{1,0:T(8,128)(2,1)} copy(bf16[384,256]{1,0:T(8,128)(2,1)S(1)} %linear_attention.1) | data formatting | bytes 393216

commit v3 on v2

--- a/solution.py
+++ b/solution.py
@@ -126,9 +126,12 @@
         loads.append(copy)
         return copy
 
+    part_rows = rows // TOKEN_PARTS
+    ld_tok = [
+        load(tok_h.at[pl.ds(i * part_rows, part_rows)], tok.at[pl.ds(i * part_rows, part_rows)])
+        for i in range(TOKEN_PARTS)
+    ]
     ld_ing = load(ing_h, ing)
-    part_rows = rows // TOKEN_PARTS
-    ld_tok = [load(tok_h.at[pl.ds(i * part_rows, part_rows)], tok.at[pl.ds(i * part_rows, part_rows)]) for i in range(TOKEN_PARTS)]
     ld_dd = load(dd_h, dd)
     ld_du = load(du_h.at[:, pl.ds(pl.multiple_of(me * QUERY_FEATURES, QUERY_FEATURES), QUERY_FEATURES)], du)
     ld_off = load(off_h, doff)
@@ -171,7 +174,7 @@
     tiles = part_rows // 16
     for i in range(TOKEN_PARTS):
         ld_tok[i].wait()
-        lax.fori_loop(i * tiles, (i + 1) * tiles, norm_rows, 0, unroll=3)
+        lax.fori_loop(i * tiles, (i + 1) * tiles, norm_rows, 0, unroll=6)
 
     ld_dd.wait()
     ld_du.wait()
@@ -180,21 +183,28 @@
     ld_wk.wait()
     ld_wv.wait()
     low = dot(nrm[...], dd[...], 1, 1).astype(bf16)
+    kk[...] = dot(nrm[...], wk[...]).astype(bf16)
     pre = dot(low, du[...]) + doff[...]
+    vv[...] = dot(nrm[...], wv[...]).astype(bf16)
     log_decay = (jnp.minimum(pre, 0.0) - jnp.log1p(jnp.exp(-jnp.abs(pre)))) / decay_temper + ext[...]
     d_hi = log_decay.astype(bf16)
     rest = log_decay - d_hi.astype(f32)
     d_mid = rest.astype(bf16)
     d_low = (rest - d_mid.astype(f32)).astype(bf16)
-    lower = lax.broadcasted_iota(jnp.int32, (rows, rows), 0) >= lax.broadcasted_iota(jnp.int32, (rows, rows), 1)
-    lower = jnp.where(lower, 1.0, 0.0).astype(bf16)
-    cum[...] = dot(lower, d_hi) + (dot(lower, d_mid) + dot(lower, d_low))
+    size = (CHUNK, CHUNK)
+    r_at, c_at = lax.broadcasted_iota(jnp.int32, size, 0), lax.broadcasted_iota(jnp.int32, size, 1)
+    lower = jnp.where(r_at >= c_at, 1.0, 0.0).astype(bf16)
+    carried = jnp.zeros((1, QUERY_FEATURES), f32)
+    for i in range(chunks):
+        own = slice(i * CHUNK, (i + 1) * CHUNK)
+        sums = dot(lower, jnp.concatenate([d_hi[own], d_mid[own], d_low[own]], axis=1))
+        sums = sums[:, :128] + (sums[:, 128:256] + sums[:, 256:]) + carried
+        cum[own, :] = sums
+        carried = sums[CHUNK - 1 :, :]
     closing = cum[rows - 1 : rows, :]
     gsend[...] = closing
     garr[y] = closing
 
-    kk[...] = dot(nrm[...], wk[...]).astype(bf16)
-    vv[...] = dot(nrm[...], wv[...]).astype(bf16)
     khat = (kk[...].astype(f32) * jnp.exp(closing - cum[...])).astype(bf16)
     state = dot(vv[...], khat, 0, 0).astype(bf16)
     st[...] = state.reshape(ny, piece, QUERY_FEATURES)
@@ -221,11 +231,11 @@
             copy.start()
 
     def tell_near(d, carry):
-        pl.semaphore_signal(ready, inc=1, device_id={"z": z - d}, device_id_type=MESH)
+        pl.semaphore_signal(ready.at[z], inc=1, device_id={"z": z - d}, device_id_type=MESH)
         return carry
 
     def tell_last(g, carry):
-        pl.semaphore_signal(ready, inc=1, device_id={"z": g * GROUP + GROUP - 1}, device_id_type=MESH)
+        pl.semaphore_signal(ready.at[z], inc=1, device_id={"z": g * GROUP + GROUP - 1}, device_id_type=MESH)
         return carry
 
     lax.fori_loop(1, place + 1, tell_near, 0)
@@ -239,8 +249,6 @@
     gate = dot(nrm[...], wg[...]).astype(bf16).astype(f32)
     fac[...] = gate * (1.0 / (1.0 + jnp.exp(-gate))) * hg[...]
 
-    size = (CHUNK, CHUNK)
-    r_at, c_at = lax.broadcasted_iota(jnp.int32, size, 0), lax.broadcasted_iota(jnp.int32, size, 1)
     mid = CHUNK // 2
     same = (r_at >= c_at) & ((r_at >= mid) == (c_at >= mid))
     cross = (r_at >= mid) & (c_at < mid)
@@ -287,17 +295,13 @@
             for src, dst, sem, got in zip((tsend, gtsend), land, send, recv)
         ]
 
-    @pl.when(reach > 0)
-    def _():
-        pl.semaphore_wait(ready, reach)
-
-    def send_near(i, carry):
-        d = GROUP - 1 - place - i
+    def send_near(d, carry):
+        pl.semaphore_wait(ready.at[z + d], 1)
         for copy in copy2(0, d, d, (s2r, g2r)):
             copy.start()
         return carry
 
-    lax.fori_loop(0, GROUP - 1 - place, send_near, 0)
+    lax.fori_loop(1, GROUP - place, send_near, 0)
 
     def take_near(d, carry):
         into, weight = carry
@@ -308,17 +312,23 @@
     nothing = (jnp.zeros((piece, QUERY_FEATURES), f32), jnp.zeros((1, QUERY_FEATURES), f32))
     near, near_weight = lax.fori_loop(1, place + 1, take_near, nothing)
 
+    groups = nz // GROUP
+
+    def send_far(g, carry):
+        for p in range(GROUP):
+            pl.semaphore_wait(ready.at[g * GROUP + p], 1)
+            for copy in copy2(1, (g - group) * GROUP + p + 1 - GROUP, group, (s2f, g2f)):
+                copy.start()
+        return carry
+
+    until = jnp.where(group == 0, 2, groups)
+
     @pl.when(last)
     def _():
         tsend[1] = (jnp.exp(total) * near + run).astype(bf16)
         gtsend[1] = near_weight + total
 
-        def send_far(d, carry):
-            for copy in copy2(1, d, group, (s2f, g2f)):
-                copy.start()
-            return carry
-
-        lax.fori_loop(1, later + 1, send_far, 0)
+        lax.fori_loop(group + 1, until, send_far, 0)
 
     def take_far(i, carry):
         into, weight = carry
@@ -345,6 +355,10 @@
     for o in far_first(ny):
         copy3(o).start()
 
+    @pl.when(last & (group == 0))
+    def _():
+        lax.fori_loop(until, groups, send_far, 0)
+
     @pl.when(first_of_all)
     def _():
         sin[pl.ds(0, ny)] = jnp.zeros((ny, piece, QUERY_FEATURES), bf16)
@@ -357,24 +371,25 @@
     come = sin[pl.ds(0, ny)].reshape(DV, QUERY_FEATURES)
 
     first, second = pl.ds(0, half), pl.ds(half, half)
+    quarters = [pl.ds(i * (half // 2), half // 2) for i in range(4)]
 
     def go(slot, part, k, where):
         return pltpu.make_async_remote_copy(
-            src_ref=gat.at[slot, part], dst_ref=gat.at[slot, part], send_sem=gs, recv_sem=gr.at[k],
+            src_ref=gat.at[slot, part], dst_ref=gat.at[slot, part], send_sem=gs.at[{0: 0, 14: 0, 2: 1, 15: 1}.get(k, 2)], recv_sem=gr.at[k],
             device_id=where, device_id_type=MESH)
 
     east, west, other = {"x": plus}, {"x": minus}, {"c": 1 - c}
     from_west, from_east, from_far = minus * 2 + c, plus * 2 + c, across * 2 + c
     twin = 1 - 2 * c
 
-    for part, sends in ((first, ((0, east), (6, other))), (second, ((2, west), (7, other)))):
+    for part, sends in ((first, ((0, 0, east), (1, 14, east))), (second, ((2, 2, west), (3, 15, west)))):
         there = att[part, :] + dot(qhat[part, :], come, 1, 1)
         scale = lax.rsqrt(jnp.mean(there * there, axis=1, keepdims=True) + norm_eps)
         gat[me, part, :] = (there * scale * fac[part, :]).astype(bf16)
-        for k, where in sends:
-            go(me, part, k, where).start()
-    go(me, second, 1, east).start()
-    go(me, first, 3, west).start()
+        for i, k, where in sends:
+            go(me, quarters[i], k, where).start()
+    go(me, first, 6, other).start()
+    go(me, second, 7, other).start()
 
     ld_wo.wait()
 
@@ -384,11 +399,32 @@
 
     add(me, first, True)
     add(me, second, True)
-    go(from_west, first, 0, west).wait_recv()
-    go(from_west, first, 4, east).start()
+    all_of(gat.at[0], half, gs.at[0])
+    go(me, second, 1, east).start()
+    all_of(gat.at[0], half, gs.at[1])
+    go(me, first, 3, west).start()
+
+    def hand_on_east():
+        for i, k, on in ((0, 0, 4), (1, 14, 16)):
+            go(from_west, quarters[i], k, west).wait_recv()
+            go(from_west, quarters[i], on, east).start()
+
+    def hand_on_west():
+        for i, k, on in ((2, 2, 5), (3, 15, 17)):
+            go(from_east, quarters[i], k, east).wait_recv()
+            go(from_east, quarters[i], on, west).start()
+
+    @pl.when(x == 1)
+    def _():
+        hand_on_west()
+        hand_on_east()
+
+    @pl.when(x != 1)
+    def _():
+        hand_on_east()
+        hand_on_west()
+
     go(from_west, first, 8, other).start()
-    go(from_east, second, 2, east).wait_recv()
-    go(from_east, second, 5, west).start()
     go(from_east, second, 9, other).start()
     go(me + twin, first, 6, other).wait_recv()
     go(me + twin, second, 7, other).wait_recv()
@@ -410,9 +446,11 @@
     add(from_west + twin, second)
     go(from_east + twin, first, 11, other).wait_recv()
     add(from_east + twin, first)
-    go(from_far, first, 4, west).wait_recv()
+    go(from_far, quarters[0], 4, west).wait_recv()
+    go(from_far, quarters[1], 16, west).wait_recv()
     go(from_far, first, 12, other).start()
-    go(from_far, second, 5, east).wait_recv()
+    go(from_far, quarters[2], 5, east).wait_recv()
+    go(from_far, quarters[3], 17, east).wait_recv()
     go(from_far, second, 13, other).start()
     add(from_far, first)
     add(from_far, second)
@@ -470,7 +508,7 @@
             all_of(zfar, count, s2s.at[1])
             all_of(zgfar, count, g2s.at[1])
 
-    all_of(gat, 7, gs)
+    all_of(gat, 6, gs.at[2])
 
 
 def local(nz, ny, *args):
@@ -522,12 +560,12 @@
         V((rows, DV), f32),
         V((8, 128), f32),
         V((2 * NX, 8, 128), f32),
-        pltpu.SemaphoreType.REGULAR,
+        pltpu.SemaphoreType.REGULAR((nz,)),
         dma((12 + TOKEN_PARTS,)),
         dma, dma, dma, dma,
         dma((2,)), dma((GROUP,)), dma((2,)), dma((GROUP,)), dma((nz // GROUP,)), dma((nz // GROUP,)),
         dma, dma,
-        dma, dma((14,)),
+        dma((3,)), dma((18,)),
         dma, dma,
     ]
     operands = (

time: 45.6 us -> 43 us (0.943)
  the two profiles are of different devices: /device:TPU:256 before, /device:TPU:65 now
where the time goes in v3:
time: 43 us; the launch traced here: 42.9 us
  Pallas kernels  42.2 us (98%)
  local copies, waits for them, and re-layouts  0.68 us (2%)
    pallas_call x1, Pallas kernels, local(): pl.pallas_call(functools.partial(kernel, nz, ny), out_shape=jax.ShapeDtyp...  42.2 us

profile of v3, /device:TPU:65, one launch (start us, length us, event | category | flops | bytes accessed | tf_op | source)
XLA Modules:
  0.0 42.9 jit_solution(10136629386462448908)
XLA Ops:
  0.0 42.2 %linear_attention.1 = bf16[384,256]{1,0:T(8,128)(2,1)S(1)} custom-call(bf16[384,2048]{1,0:T(8,128)(2,1)} %tok_h.1, f32[1,2048]{1,0:T(1,128)} %bitcast.6, bf16[2048,128]{1,0:T(8,128)(2,1)} %wq_h.1, bf16[2048,128]{1,0:T(8,128)(2,1)} %wk_h.1, bf16[2048,256]{1,0:T(8,128)(2,1)} %wv_h.1, bf16[2048,256]{1,0:T(8,128)(2,1)} %wg_h.1, bf16[32,2048]{1,0:T(8,128)(2,1)} %bitcast.5, ...), custom_call_target="tpu_custom_call" | custom-call | tf_op jit(solution)/shard_map/linear_attention/pallas_call | solution.py:575
  42.2 0.7 %copy.15 = bf16[384,256]{1,0:T(8,128)(2,1)} copy(bf16[384,256]{1,0:T(8,128)(2,1)S(1)} %linear_attention.1) | data formatting | bytes 393216

commit v4 on v3

--- a/solution.py
+++ b/solution.py
@@ -375,7 +375,7 @@
 
     def go(slot, part, k, where):
         return pltpu.make_async_remote_copy(
-            src_ref=gat.at[slot, part], dst_ref=gat.at[slot, part], send_sem=gs.at[{0: 0, 14: 0, 2: 1, 15: 1}.get(k, 2)], recv_sem=gr.at[k],
+            src_ref=gat.at[slot, part], dst_ref=gat.at[slot, part], send_sem=gs.at[0 if k in (6, 7) else 1], recv_sem=gr.at[k],
             device_id=where, device_id_type=MESH)
 
     east, west, other = {"x": plus}, {"x": minus}, {"c": 1 - c}
@@ -399,9 +399,8 @@
 
     add(me, first, True)
     add(me, second, True)
-    all_of(gat.at[0], half, gs.at[0])
+    all_of(gat.at[0], rows, gs.at[0])
     go(me, second, 1, east).start()
-    all_of(gat.at[0], half, gs.at[1])
     go(me, first, 3, west).start()
 
     def hand_on_east():
@@ -426,10 +425,6 @@
 
     go(from_west, first, 8, other).start()
     go(from_east, second, 9, other).start()
-    go(me + twin, first, 6, other).wait_recv()
-    go(me + twin, second, 7, other).wait_recv()
-    add(me + twin, first)
-    add(me + twin, second)
     add(from_west, first)
     add(from_east, second)
     go(from_west, second, 1, west).wait_recv()
@@ -438,20 +433,18 @@
     go(from_east, first, 11, other).start()
     add(from_west, second)
     add(from_east, first)
-    go(from_west + twin, first, 8, other).wait_recv()
-    add(from_west + twin, first)
-    go(from_east + twin, second, 9, other).wait_recv()
-    add(from_east + twin, second)
-    go(from_west + twin, second, 10, other).wait_recv()
-    add(from_west + twin, second)
-    go(from_east + twin, first, 11, other).wait_recv()
-    add(from_east + twin, first)
     go(from_far, quarters[0], 4, west).wait_recv()
     go(from_far, quarters[1], 16, west).wait_recv()
     go(from_far, first, 12, other).start()
     go(from_far, quarters[2], 5, east).wait_recv()
     go(from_far, quarters[3], 17, east).wait_recv()
     go(from_far, second, 13, other).start()
+    for slot, part, k in (
+        (me, first, 6), (me, second, 7), (from_west, first, 8), (from_east, second, 9),
+        (from_west, second, 10), (from_east, first, 11),
+    ):
+        go(slot + twin, part, k, other).wait_recv()
+        add(slot + twin, part)
     add(from_far, first)
     add(from_far, second)
     go(from_far + twin, first, 12, other).wait_recv()
@@ -508,7 +501,7 @@
             all_of(zfar, count, s2s.at[1])
             all_of(zgfar, count, g2s.at[1])
 
-    all_of(gat, 6, gs.at[2])
+    all_of(gat, 6, gs.at[1])
 
 
 def local(nz, ny, *args):
@@ -565,7 +558,7 @@
         dma, dma, dma, dma,
         dma((2,)), dma((GROUP,)), dma((2,)), dma((GROUP,)), dma((nz // GROUP,)), dma((nz // GROUP,)),
         dma, dma,
-        dma((3,)), dma((18,)),
+        dma((2,)), dma((18,)),
         dma, dma,
     ]
     operands = (

time: 43 us -> 42.9 us (level)
  no operation moved by 1% of the time
where the time goes in v4:
time: 42.9 us; the launch traced here: 42.7 us
  Pallas kernels  42 us (98%)
  local copies, waits for them, and re-layouts  0.68 us (2%)
    pallas_call x1, Pallas kernels, local(): pl.pallas_call(functools.partial(kernel, nz, ny), out_shape=jax.ShapeDtyp...  42 us

profile of v4, /device:TPU:65, one launch (start us, length us, event | category | flops | bytes accessed | tf_op | source)
XLA Modules:
  0.0 42.7 jit_solution(13740249466775041902)
XLA Ops:
  0.0 42.0 %linear_attention.1 = bf16[384,256]{1,0:T(8,128)(2,1)S(1)} custom-call(bf16[384,2048]{1,0:T(8,128)(2,1)} %tok_h.1, f32[1,2048]{1,0:T(1,128)} %bitcast.6, bf16[2048,128]{1,0:T(8,128)(2,1)} %wq_h.1, bf16[2048,128]{1,0:T(8,128)(2,1)} %wk_h.1, bf16[2048,256]{1,0:T(8,128)(2,1)} %wv_h.1, bf16[2048,256]{1,0:T(8,128)(2,1)} %wg_h.1, bf16[32,2048]{1,0:T(8,128)(2,1)} %bitcast.5, ...), custom_call_target="tpu_custom_call" | custom-call | tf_op jit(solution)/shard_map/linear_attention/pallas_call | solution.py:568
  42.0 0.7 %copy.15 = bf16[384,256]{1,0:T(8,128)(2,1)} copy(bf16[384,256]{1,0:T(8,128)(2,1)S(1)} %linear_attention.1) | data formatting | bytes 393216
